TPU v7x, 32 devices: a whole 2x2x4 slice. The times are simulated.
32 devices in a mesh: fs: 8 (over z, core), tp: 4 (over y, x).
Axes of the slice: x: 2, y: 2, z: 4, core: 2. Of those that a mesh axis runs over, the one named last changes fastest.
Arguments:
- normed_in: bfloat16 [8192, 2048], P('fs'), may hold values from -6 to 6
- grad_x: bfloat16 [8192, 2048], P('fs', 'tp'), may hold values from -0.088388348 to 0.088388348
- grad_y: bfloat16 [8192, 2048], P('fs', 'tp'), may hold values from -0.088388348 to 0.088388348
- weight_x: float32 [2048, 2048], P('fs', 'tp'), may hold values from -0.125 to 0.125
- weight_y: float32 [2048, 2048], P('fs', 'tp'), may hold values from -0.125 to 0.125
- factor_x: bfloat16 [2048, 512], P('fs'), may hold values from -0.13258252 to 0.13258252
- factor_y: bfloat16 [2048, 512], P('fs'), may hold values from -0.13258252 to 0.13258252
- first_x: float32 [512, 2048], P('fs', 'tp'), may hold values from -8 to 8
- first_y: float32 [512, 2048], P('fs', 'tp'), may hold values from -8 to 8
- second_x: float32 [512, 2048], P('fs', 'tp'), may hold values from 0.5 to 2
- second_y: float32 [512, 2048], P('fs', 'tp'), may hold values from 0.5 to 2
Outputs:
- new_weight_x: float32 [2048, 2048], P('fs', 'tp')
- new_weight_y: float32 [2048, 2048], P('fs', 'tp')
- step_x: float32 [2048, 2048], P('fs', 'tp')
- step_y: float32 [2048, 2048], P('fs', 'tp')
- new_first_x: float32 [512, 2048], P('fs', 'tp')
- new_first_y: float32 [512, 2048], P('fs', 'tp')
- new_second_x: float32 [512, 2048], P('fs', 'tp')
- new_second_y: float32 [512, 2048], P('fs', 'tp')
- copy_x: bfloat16 [2048, 2048], P(None, 'tp')
- copy_y: bfloat16 [2048, 2048], P(None, 'tp')
All inputs are finite; a program needn't handle non-finite values.
Results may differ from a plain program's by a relative error of at most 0.02.
Values may be sent and summed in bfloat16 or wider, within the bound.
A program may use at most 128 MiB of HBM per device.

v0:
```python
import jax
import jax.numpy as jnp
from jax import lax
from jax.sharding import PartitionSpec as P

D = 2048
RW = 2048


def on_device(
    normed_in,
    grad_x,
    grad_y,
    weight_x,
    weight_y,
    factor_x,
    factor_y,
    first_x,
    first_y,
    second_x,
    second_y,
):
    width = grad_x.shape[1]
    contract = (((0,), (0,)), ((), ()))
    highest = lax.Precision.HIGHEST
    cotangent = jnp.concatenate((grad_x, grad_y), 1)
    summed = lax.psum_scatter(
        lax.dot_general(normed_in, cotangent, contract, preferred_element_type=jnp.float32).astype(
            jnp.bfloat16
        ),
        "fs",
        scatter_dimension=0,
        tiled=True,
    ).astype(jnp.float32)
    part_x = factor_x.astype(jnp.float32)
    part_y = factor_y.astype(jnp.float32)
    low_x = lax.dot_general(part_x, summed[:, :width], contract, precision=highest)
    low_y = lax.dot_general(part_y, summed[:, width:], contract, precision=highest)
    projected = lax.psum_scatter(
        jnp.concatenate((low_x, low_y), 1), "fs", scatter_dimension=0, tiled=True
    )
    low_x = projected[:, :width]
    low_y = projected[:, width:]
    new_first_x = 0.8 * first_x + 0.2 * low_x
    new_first_y = 0.8 * first_y + 0.2 * low_y
    new_second_x = 0.9 * second_x + 0.1 * low_x * low_x
    new_second_y = 0.9 * second_y + 0.1 * low_y * low_y
    direction = jnp.concatenate(
        (new_first_x / jnp.sqrt(new_second_x), new_first_y / jnp.sqrt(new_second_y)), 1
    )
    piece = lax.all_gather(direction, "fs", axis=0, tiled=True)
    part_x = factor_x.astype(jnp.float32)
    part_y = factor_y.astype(jnp.float32)
    update_x = jnp.dot(part_x, piece[:, :width], precision=highest)
    update_y = jnp.dot(part_y, piece[:, width:], precision=highest)
    total = lax.psum(jnp.sum(update_x * update_x) + jnp.sum(update_y * update_y), ("fs", "tp"))
    scale = jnp.minimum(1.0, 0.25 * jnp.sqrt(2.0 * D * RW) / jnp.sqrt(total))
    step_x = scale * update_x
    step_y = scale * update_y
    new_x = weight_x - 0.02 * step_x
    new_y = weight_y - 0.02 * step_y
    copy_x, copy_y = (
        lax.all_gather(new_x.astype(jnp.bfloat16), "fs", axis=0, tiled=True),
        lax.all_gather(new_y.astype(jnp.bfloat16), "fs", axis=0, tiled=True),
    )
    return (
        new_x,
        new_y,
        step_x,
        step_y,
        new_first_x,
        new_first_y,
        new_second_x,
        new_second_y,
        copy_x,
        copy_y,
    )


def solution(mesh):
    in_specs = (
        P("fs", None),
        P("fs", "tp"),
        P("fs", "tp"),
        P("fs", "tp"),
        P("fs", "tp"),
        P("fs", None),
        P("fs", None),
        P("fs", "tp"),
        P("fs", "tp"),
        P("fs", "tp"),
        P("fs", "tp"),
    )
    out_specs = (
        P("fs", "tp"),
        P("fs", "tp"),
        P("fs", "tp"),
        P("fs", "tp"),
        P("fs", "tp"),
        P("fs", "tp"),
        P("fs", "tp"),
        P("fs", "tp"),
        P(None, "tp"),
        P(None, "tp"),
    )
    return jax.shard_map(
        on_device, mesh=mesh, in_specs=in_specs, out_specs=out_specs, check_vma=False
    )
```

profile of v0, /device:TPU:0, one launch (start us, length us, event | category | flops | bytes accessed | tf_op | source)
XLA Modules:
  0.0 260.1 jit_solution(1484371934440592451)
XLA Ops:
  7.2 9.4 %convert_bitcast_fusion = bf16[2048,1024]{0,1:T(8,128)(2,1)} fusion(bf16[1024,2048]{1,0:T(8,128)(2,1)} %param.11, bf16[1024,512]{1,0:T(8,128)(2,1)} %param.13, bf16[1024,512]{1,0:T(8,128)(2,1)} %param.12), kind=kOutput, calls=%fused_computation | convolution fusion | flops 4301258752 | bytes 10485760 | tf_op jit(solution)/shard_map/dot_general | solution.py:28
  16.7 52.8 %reduce-scatter.5.cloned.1.call-done = bf16[256,1024]{0,1:T(8,128)(2,1)} async-done(((bf16[2048,1024]{0,1:T(8,128)(2,1)}), bf16[256,1024]{0,1:T(8,128)(2,1)}) %reduce-scatter.5.cloned.1.call-update) | async-done | bytes 524304 | tf_op jit(solution)/shard_map/reduce_scatter | solution.py:27
  69.5 1.2 convolution_bitcast_fusion
  70.7 1.2 convolution_bitcast_fusion.1
  72.1 1.8 copy.64
  74.0 34.6 %reduce-scatter.7.cloned.1.call-done = f32[64,1024]{1,0:T(8,128)} async-done(((f32[512,1024]{1,0:T(8,128)}), f32[64,1024]{1,0:T(8,128)}) %reduce-scatter.7.cloned.1.call-update) | async-done | bytes 262160 | tf_op jit(solution)/shard_map/reduce_scatter | solution.py:39
  108.7 1.8 rsqrt_multiply_fusion.1
  110.5 0.7 pad_maximum_fusion.1
  111.3 27.7 %all-gather.4.cloned.1.call-done = f32[512,1024]{1,0:T(8,128)} async-done(((f32[64,1024]{1,0:T(8,128)}), f32[512,1024]{1,0:T(8,128)}) %all-gather.4.cloned.1.call-update) | async-done | bytes 2097168 | tf_op jit(solution)/shard_map/all_gather | solution.py:51
  139.0 2.8 %multiply_reduce_fusion = (f32[]{:T(128)}, f32[512,256]{1,0:T(8,128)S(1)}) fusion(bf16[256,512]{1,0:T(8,128)(2,1)S(1)} %copy-done, f32[512,1024]{1,0:T(8,128)} %all-gather.4.cloned.1.call-done), kind=kOutput, calls=%fused_computation.15 | convolution fusion | flops 805568512 | bytes 1835012 | tf_op jit(solution)/shard_map/dot_general | solution.py:55
  141.8 2.8 %multiply_reduce_fusion.1 = (f32[]{:T(128)}, f32[512,256]{1,0:T(8,128)S(1)}) fusion(bf16[256,512]{1,0:T(8,128)(2,1)S(1)} %copy-done.1, f32[512,1024]{1,0:T(8,128)} %all-gather.4.cloned.1.call-done), kind=kOutput, calls=%fused_computation.16 | convolution fusion | flops 805568512 | bytes 1835012 | tf_op jit(solution)/shard_map/dot_general | solution.py:54
  146.0 0.2 copy.57
  146.2 40.2 %psum.7 = f32[]{:T(128)} all-reduce(f32[]{:T(128)S(6)} %add.25), channel_id=1, replica_groups=mesh['fs'=8,'tp'=4] {'fs','tp'}, use_global_device_ids=true, to_apply=%region_4.0 | all-reduce | flops 1 | bytes 8 | tf_op jit(solution)/shard_map/psum | solution.py:56
  187.0 0.8 fusion.12
  187.9 1.2 copy.56
  189.1 0.8 fusion.13
  190.0 1.0 copy.58
  190.9 1.0 copy.60
  191.9 1.0 copy.59
  192.9 1.0 copy.61
  193.9 24.1 %all-gather.8.cloned.1.call-done = bf16[2048,512]{0,1:T(8,128)(2,1)} async-done(((bf16[256,512]{0,1:T(8,128)(2,1)}), bf16[2048,512]{0,1:T(8,128)(2,1)}) %all-gather.8.cloned.1.call-update) | async-done | bytes 2097168 | tf_op jit(solution)/shard_map/all_gather | solution.py:64
  218.0 3.9 %copy.63 = bf16[2048,512]{1,0:T(8,128)(2,1)} copy(bf16[2048,512]{0,1:T(8,128)(2,1)} %all-gather.8.cloned.1.call-done) | data formatting | bytes 4194304
  221.9 27.8 %all-gather.6.cloned.1.call-done = bf16[2048,512]{0,1:T(8,128)(2,1)} async-done(((bf16[256,512]{0,1:T(8,128)(2,1)}), bf16[2048,512]{0,1:T(8,128)(2,1)}) %all-gather.6.cloned.1.call-update) | async-done | bytes 2097168 | tf_op jit(solution)/shard_map/all_gather | solution.py:63
  249.7 3.9 %copy.62 = bf16[2048,512]{1,0:T(8,128)(2,1)} copy(bf16[2048,512]{0,1:T(8,128)(2,1)} %all-gather.6.cloned.1.call-done) | data formatting | bytes 4194304
  (25 shorter events, 0.5 us)
Async XLA Ops:
  7.2 62.3 %copy-start = (bf16[256,512]{1,0:T(8,128)(2,1)S(1)}, bf16[256,512]{1,0:T(8,128)(2,1)}, u32[]{:S(2)}) copy-start(bf16[256,512]{1,0:T(8,128)(2,1)} %param.17) | copy-start | bytes 786436
  7.2 62.3 %reduce-scatter.5.cloned.1.call-start = ((), (), s32[]{:S(2)}) async-start(), calls=%async_computation.2 | async-start | bytes 4718592 | tf_op jit(solution)/shard_map/reduce_scatter | solution.py:27
  16.6 54.1 %copy-start.1 = (bf16[256,512]{1,0:T(8,128)(2,1)S(1)}, bf16[256,512]{1,0:T(8,128)(2,1)}, u32[]{:S(2)}) copy-start(bf16[256,512]{1,0:T(8,128)(2,1)} %param.16) | copy-start | bytes 786436
  16.6 92.0 %reduce-scatter.7.cloned.1.call-start = ((), (), s32[]{:S(2)}) async-start(), calls=%async_computation.6 | async-start | bytes 2359296 | tf_op jit(solution)/shard_map/reduce_scatter | solution.py:39
  73.9 34.7 %copy-start.3 = (f32[64,512]{1,0:T(8,128)S(1)}, f32[64,512]{1,0:T(8,128)}, u32[]{:S(2)}) copy-start(f32[64,512]{1,0:T(8,128)} %param.20) | copy-start | bytes 393220
  73.9 34.7 %copy-start.4 = (f32[64,512]{1,0:T(8,128)S(1)}, f32[64,512]{1,0:T(8,128)}, u32[]{:S(2)}) copy-start(f32[64,512]{1,0:T(8,128)} %param.18) | copy-start | bytes 393220
  73.9 34.7 %copy-start.5 = (f32[64,512]{1,0:T(8,128)S(1)}, f32[64,512]{1,0:T(8,128)}, u32[]{:S(2)}) copy-start(f32[64,512]{1,0:T(8,128)} %param.21) | copy-start | bytes 393220
  74.0 34.7 %copy-start.6 = (f32[64,512]{1,0:T(8,128)S(1)}, f32[64,512]{1,0:T(8,128)}, u32[]{:S(2)}) copy-start(f32[64,512]{1,0:T(8,128)} %param.19) | copy-start | bytes 393220
  74.0 65.0 %all-gather.4.cloned.1.call-start = ((), (), s32[]{:S(2)}) async-start(), calls=%async_computation.3 | async-start | bytes 2359296 | tf_op jit(solution)/shard_map/all_gather | solution.py:51
  111.2 34.7 %copy-start.2 = (f32[256,512]{1,0:T(8,128)S(1)}, f32[256,512]{1,0:T(8,128)}, u32[]{:S(2)}) copy-start(f32[256,512]{1,0:T(8,128)} %param.15) | copy-start | bytes 1572868
  111.2 106.8 %all-gather.8.cloned.1.call-start = ((), (), s32[]{:S(2)}) async-start(), calls=%async_computation.5 | async-start | bytes 2359296 | tf_op jit(solution)/shard_map/all_gather | solution.py:64
  187.8 61.9 %all-gather.6.cloned.1.call-start = ((), (), s32[]{:S(2)}) async-start(), calls=%async_computation.4 | async-start | bytes 2359296 | tf_op jit(solution)/shard_map/all_gather | solution.py:63
Sparse Core Ops, SparseCore 0:
  16.8 52.6 reduce-scatter.4
  74.1 34.5 reduce-scatter.6
  111.3 27.5 all-gather.3
  187.9 30.0 all-gather.7
  220.0 29.6 all-gather.5
where the time goes:
time: 261 us; the launch traced here: 260 us
  waiting for transfers between devices  167 us (64%)
  blocking collectives  40.2 us (15%)
  matrix products  17.5 us (7%)
  between operations  15.9 us (6%)
  local copies, waits for them, and re-layouts  15.1 us (6%)
  other arithmetic  4.31 us (2%)
    reduce_scatter x1, waiting for transfers between devices, on_device(): lax.psum_scatter(lax.dot_general(normed_in, cotangent, contract, preferre...  52.8 us
    psum x1, blocking collectives, on_device(): lax.psum(jnp.sum(update_x * update_x) + jnp.sum(update_y * update_y), ('f...  40.2 us
    reduce_scatter x1, waiting for transfers between devices, on_device(): lax.psum_scatter(jnp.concatenate((low_x, low_y), 1), 'fs', scatter_dimens...  34.6 us
    all_gather x1, waiting for transfers between devices, on_device(): lax.all_gather(new_x.astype(jnp.bfloat16), 'fs', axis=0, tiled=True)  27.8 us
    all_gather x1, waiting for transfers between devices, on_device(): piece = lax.all_gather(direction, 'fs', axis=0, tiled=True)  27.7 us
    all_gather x1, waiting for transfers between devices, on_device(): lax.all_gather(new_y.astype(jnp.bfloat16), 'fs', axis=0, tiled=True)  24.1 us
    unnamed x23, local copies, waits for them, and re-layouts  15.1 us
    dot_general x1, matrix products, on_device(): lax.dot_general(normed_in, cotangent, contract, preferred_element_type=jn...  9.38 us
  transfers between devices with their start and end apart: 5, of which 5 were waited for; matrix products, arithmetic and copies ran while one was open for 4% of the time, Pallas kernels for 0%

commit v1 on v0

v1 whole, which is shorter than its diff:
```python
import functools
import math

import jax
import jax.numpy as jnp
from jax import lax
from jax.experimental import pallas as pl
from jax.experimental.pallas import tpu as pltpu
from jax.sharding import PartitionSpec as P

MESH = pl.DeviceIdType.MESH
F32, BF16 = jnp.float32, jnp.bfloat16
ROWS = (((0,), (0,)), ((), ()))


def exchange_kernel(
    nfs,
    ntp,
    normed,
    grad_x,
    grad_y,
    weight_x,
    weight_y,
    factor_x,
    factor_y,
    first_x,
    first_y,
    second_x,
    second_y,
    f_out,
    w_out,
    d_out,
    low_out,
    tot_out,
    n_buf,
    gx_buf,
    gy_buf,
    f_buf,
    h_buf,
    low,
    sib,
    rs_send,
    rs_recv,
    d_buf,
    w_buf,
    w16,
    fm,
    sm,
    g_hi,
    g_lo,
    tot_recv,
    lsem,
    bar_sem,
    f_line_s,
    f_line_r,
    f_tp_s,
    f_tp_r,
    f_sib_s,
    f_sib_r,
    f_own_s,
    w_s,
    w_r,
    w_sib_s,
    w_sib_r,
    sib_s,
    rs_s,
    rs_r,
    d_line_s,
    d_line_r,
    d_sib_s,
    d_sib_r,
    t_s,
    t_r,
):
    nz = nfs // 2
    i = lax.axis_index("fs")
    t = lax.axis_index("tp")
    z, c = i // 2, lax.rem(i, 2)
    o = z * 2 + 1 - c
    R, rank = factor_x.shape
    tokens, w = gx_buf.shape
    r = rank // nfs
    q = math.gcd(ntp, R // 16)
    rq = R // q
    u, g0 = lax.rem(t, q), t // q * q

    def local(src, dst, k):
        cp = pltpu.make_async_copy(src, dst, lsem.at[k])
        cp.start()
        return cp

    def send(src, dst, s, rr, dev):
        return pltpu.make_async_remote_copy(
            src_ref=src, dst_ref=dst, send_sem=s, recv_sem=rr, device_id=dev, device_id_type=MESH
        )

    def rows(k, n):
        return pl.ds(pl.multiple_of(k * n, n), n)

    cps_f = [
        local(factor_x, f_buf.at[0, rows(i, R)], 0),
        local(factor_y, f_buf.at[1, rows(i, R)], 1),
    ]
    cps_w = [
        local(weight_x, w_buf.at[:, pl.ds(0, w)], 2),
        local(weight_y, w_buf.at[:, pl.ds(w, w)], 3),
    ]
    cps_n = [local(normed, n_buf, 4), local(grad_x, gx_buf, 5), local(grad_y, gy_buf, 6)]
    cps_m = [
        local(first_x, fm.at[:, pl.ds(0, w)], 7),
        local(first_y, fm.at[:, pl.ds(w, w)], 8),
        local(second_x, sm.at[:, pl.ds(0, w)], 9),
        local(second_y, sm.at[:, pl.ds(w, w)], 10),
    ]

    barrier = pltpu.get_barrier_semaphore()
    peers = [{"fs": lax.rem(z + k, nz) * 2 + c} for k in range(1, nz)] + [{"fs": o}]
    peers += [{"tp": lax.rem(t + k, ntp)} for k in range(1, ntp)]
    for dev in peers:
        pl.semaphore_signal(barrier, inc=1, device_id=dev, device_id_type=MESH)
    pl.semaphore_wait(barrier, len(peers))
    for cp in cps_f:
        cp.wait()

    sent = []

    def go(cp):
        cp.start()
        sent.append(cp)

    def piece(src_fs, part):
        return f_buf.at[:, pl.ds(pl.multiple_of(src_fs * R + part * rq, rq), rq)]

    own = piece(i, u)
    for k in range(1, nz):
        zd = lax.rem(z + k, nz)
        go(send(own, own, f_line_s.at[k], f_line_r.at[z], {"fs": zd * 2 + c}))
    mine = f_buf.at[:, rows(i, R)]
    go(send(mine, mine, f_own_s.at[0], f_sib_r.at[z, 0], {"fs": o}))

    for cp in cps_w:
        cp.wait()
    w16[...] = w_buf[...].astype(BF16)
    put = local(w16, w_out.at[rows(i, R)], 2)

    def w_hop(step):
        for side, sign in ((0, 1), (1, -1)):
            src = z - sign * step
            nxt = z + sign
            has = (src >= 0) & (src < nz)
            to = has & (nxt >= 0) & (nxt < nz)
            slot = w_out.at[rows(src * 2 + c, R)]

            if step:

                @pl.when(has)
                def _():
                    send(slot, slot, w_s.at[0, side], w_r.at[src], {"fs": o}).wait_recv()
                    send(slot, slot, w_sib_s.at[src], w_sib_r.at[src], {"fs": o}).start()

            @pl.when(to)
            def _():
                a = slot if step else w16
                send(a, slot, w_s.at[step, side], w_r.at[src], {"fs": nxt * 2 + c}).start()

    w_hop(0)
    w_own = w_out.at[rows(i, R)]
    go(send(w16, w_own, w_sib_s.at[z], w_sib_r.at[z], {"fs": o}))

    for k in range(1, nz):
        zs = lax.rem(z + nz - k, nz)
        p = piece(zs * 2 + c, u)
        send(p, p, f_line_s.at[k], f_line_r.at[zs], {"fs": o}).wait_recv()
        for v in range(1, q):
            go(send(p, p, f_tp_s.at[zs, v], f_tp_r.at[zs, u], {"tp": g0 + lax.rem(u + v, q)}))
        go(send(p, p, f_sib_s.at[zs, 0], f_sib_r.at[zs, u], {"fs": o}))
    for k in range(1, nz):
        zs = lax.rem(z + nz - k, nz)
        for v in range(1, q):
            part = lax.rem(u + v, q)
            p = piece(zs * 2 + c, part)
            send(p, p, f_tp_s.at[zs, v], f_tp_r.at[zs, part], {"fs": o}).wait_recv()
            go(send(p, p, f_sib_s.at[zs, v], f_sib_r.at[zs, part], {"fs": o}))
    theirs = f_buf.at[:, rows(o, R)]
    send(theirs, theirs, f_own_s.at[0], f_sib_r.at[z, 0], {"fs": o}).wait_recv()
    for k in range(1, nz):
        zs = lax.rem(z + nz - k, nz)
        for v in range(q):
            p = piece(zs * 2 + 1 - c, v)
            send(p, p, f_sib_s.at[zs, v], f_sib_r.at[zs, v], {"fs": o}).wait_recv()
    keep_f = local(f_buf, f_out, 0)

    for cp in cps_n:
        cp.wait()
    tile = min(256, tokens)

    @pl.loop(0, tokens // tile)
    def _(k):
        a = n_buf[rows(k, tile), :]
        for b in range(2):
            h = jnp.dot(a, f_buf[b], preferred_element_type=F32)
            h_buf[rows(k, tile), pl.ds(b * rank, rank)] = h.astype(BF16)

    lanes = 128
    m = lanes // (2 * r)

    @pl.loop(0, rank // lanes)
    def _(k):
        for b, g in ((0, gx_buf), (1, gy_buf)):
            h = h_buf[:, pl.ds(pl.multiple_of(b * rank + k * lanes, lanes), lanes)]
            part = lax.dot_general(h, g[...], ROWS, preferred_element_type=F32)
            low[pl.ds(k * m, m), :, :, pl.ds(b * w, w)] = part.reshape(m, 2, r, w)

    go(send(low.at[:, 1 - c], sib, sib_s.at[0], sib_s.at[1], {"fs": o}))
    sent[-1].wait_recv()
    for k in range(1, nz):
        zd = lax.rem(z + k, nz)
        rs_send[zd] = (low[zd, c] + sib[zd]).astype(BF16)
        go(send(rs_send.at[zd], rs_recv.at[z], rs_s.at[k], rs_r.at[z], {"fs": zd * 2 + c}))

    for step in range(1, nz - 1):
        w_hop(step)

    @pl.loop(0, rank // lanes)
    def _(k):
        for b in range(2):
            cols = pl.ds(pl.multiple_of(k * lanes, lanes), lanes)
            gram = lax.dot_general(f_buf[b, :, cols], f_buf[b], ROWS, preferred_element_type=F32)
            hi = gram.astype(BF16)
            g_hi[b, rows(k, lanes), :] = hi
            g_lo[b, rows(k, lanes), :] = (gram - hi.astype(F32)).astype(BF16)

    for cp in cps_m:
        cp.wait()
    total = low[z, c] + sib[z]
    for k in range(1, nz):
        zs = lax.rem(z + k, nz)
        send(rs_recv.at[zs], rs_recv.at[zs], rs_s.at[k], rs_r.at[zs], {"fs": o}).wait_recv()
        total = total + rs_recv[zs].astype(F32)
    low_out[...] = total
    nf = 0.8 * fm[...] + 0.2 * total
    ns = 0.9 * sm[...] + 0.1 * total * total
    d_buf[rows(i, r), :] = (nf / jnp.sqrt(ns)).astype(BF16)

    d_own = d_buf.at[rows(i, r)]
    for k in range(1, nz):
        zd = lax.rem(z + k, nz)
        go(send(d_own, d_own, d_line_s.at[k], d_line_r.at[z], {"fs": zd * 2 + c}))
    go(send(d_own, d_own, d_sib_s.at[z], d_sib_r.at[z], {"fs": o}))
    for k in range(1, nz):
        zs = lax.rem(z + k, nz)
        p = d_buf.at[rows(zs * 2 + c, r)]
        send(p, p, d_line_s.at[k], d_line_r.at[zs], {"fs": o}).wait_recv()
        go(send(p, p, d_sib_s.at[zs], d_sib_r.at[zs], {"fs": o}))
    for k in range(nz):
        zs = lax.rem(z + k, nz)
        p = d_buf.at[rows(zs * 2 + 1 - c, r)]
        send(p, p, d_sib_s.at[zs], d_sib_r.at[zs], {"fs": o}).wait_recv()
    keep_d = local(d_buf, d_out, 1)

    part = 0.0
    for b in range(2):
        d = d_buf[:, pl.ds(b * w, w)]
        gd = jnp.dot(g_hi[b], d, preferred_element_type=F32)
        gd = gd + jnp.dot(g_lo[b], d, preferred_element_type=F32)
        part = part + jnp.sum(gd * d.astype(F32))
    tot_recv[t] = jnp.full(tot_recv.shape[1:], part, F32)
    for k in range(1, ntp):
        slot = tot_recv.at[t]
        go(send(slot, slot, t_s.at[k], t_r.at[t], {"tp": lax.rem(t + k, ntp)}))

    if nz > 1:
        w_hop(nz - 1)

    acc = tot_recv[t]
    for k in range(1, ntp):
        ts = lax.rem(t + k, ntp)
        slot = tot_recv.at[ts]
        send(slot, slot, t_s.at[k], t_r.at[ts], {"fs": o}).wait_recv()
        acc = acc + tot_recv[ts]
    tot_out[...] = acc

    for zs in range(nz):
        slot = w_out.at[pl.ds((zs * 2) * R, R)]
        send(slot, slot, w_sib_s.at[zs], w_sib_r.at[zs], {"fs": o}).wait_recv()

        @pl.when(zs != z)
        def _():
            send(slot, slot, w_sib_s.at[zs], w_sib_r.at[zs], {"fs": o}).wait_send()

    for step in range(nz - 1):
        for side, sign in ((0, 1), (1, -1)):
            src = z - sign * step
            nxt = z + sign

            @pl.when((src >= 0) & (src < nz) & (nxt >= 0) & (nxt < nz))
            def _():
                a = w_out.at[rows(src * 2 + c, R)] if step else w16
                send(a, a, w_s.at[step, side], w_r.at[0], {"fs": o}).wait_send()

    for cp in sent:
        cp.wait_send()
    put.wait()
    keep_f.wait()
    keep_d.wait()


def output_kernel(
    scale_top,
    f_full,
    w_full,
    d,
    low,
    tot,
    weight_x,
    weight_y,
    factor_x,
    factor_y,
    first_x,
    first_y,
    second_x,
    second_y,
    new_x,
    new_y,
    step_x,
    step_y,
    nf_x,
    nf_y,
    ns_x,
    ns_y,
    copy_x,
    copy_y,
):
    scale = jnp.minimum(1.0, scale_top / jnp.sqrt(tot[0:1, 0:1]))
    w = weight_x.shape[1]
    sides = (
        (factor_x, weight_x, first_x, second_x, new_x, step_x, nf_x, ns_x, copy_x),
        (factor_y, weight_y, first_y, second_y, new_y, step_y, nf_y, ns_y, copy_y),
    )
    for b, (factor, weight, first, second, new, step, nf, ns, copy) in enumerate(sides):
        cols = pl.ds(b * w, w)
        db = d[:, cols]
        up = jnp.dot(f_full[b], db, preferred_element_type=F32)
        copy[...] = (w_full[:, cols].astype(F32) - 0.02 * (scale * up)).astype(BF16)
        st = scale * jnp.dot(factor[...], db, preferred_element_type=F32)
        step[...] = st
        new[...] = weight[...] - 0.02 * st

        @pl.when(pl.program_id(0) == 0)
        def _():
            lo = low[:, cols]
            nf[...] = 0.8 * first[...] + 0.2 * lo
            ns[...] = 0.9 * second[...] + 0.1 * lo * lo


def on_device(nfs, ntp, normed, gx, gy, wx, wy, fx, fy, mx, my, sx, sy):
    tokens, depth = normed.shape
    w = gx.shape[1]
    R, rank = fx.shape
    r = rank // nfs
    nz = nfs // 2
    q = math.gcd(ntp, R // 16)
    anyspec = pl.BlockSpec(memory_space=pl.ANY)
    vmem = pl.BlockSpec(memory_space=pltpu.VMEM)
    dma = pltpu.SemaphoreType.DMA
    sds = jax.ShapeDtypeStruct
    V = pltpu.VMEM
    f_full, w_full, d, low, tot = pl.pallas_call(
        functools.partial(exchange_kernel, nfs, ntp),
        out_shape=(
            sds((2, depth, rank), BF16),
            sds((depth, 2 * w), BF16),
            sds((rank, 2 * w), BF16),
            sds((r, 2 * w), F32),
            sds((8, 128), F32),
        ),
        in_specs=[anyspec] * 11,
        out_specs=(anyspec, anyspec, anyspec, vmem, vmem),
        scratch_shapes=[
            V((tokens, depth), BF16),
            V((tokens, w), BF16),
            V((tokens, w), BF16),
            V((2, depth, rank), BF16),
            V((tokens, 2 * rank), BF16),
            V((nz, 2, r, 2 * w), F32),
            V((nz, r, 2 * w), F32),
            V((nz, r, 2 * w), BF16),
            V((nz, r, 2 * w), BF16),
            V((rank, 2 * w), BF16),
            V((R, 2 * w), F32),
            V((R, 2 * w), BF16),
            V((r, 2 * w), F32),
            V((r, 2 * w), F32),
            V((2, rank, rank), BF16),
            V((2, rank, rank), BF16),
            V((ntp, 8, 128), F32),
            dma((11,)),
            pltpu.SemaphoreType.REGULAR,
            dma((nz,)),
            dma((nz,)),
            dma((nz, q)),
            dma((nz, q)),
            dma((nz, q)),
            dma((nz, q)),
            dma((1,)),
            dma((nz, 2)),
            dma((nz,)),
            dma((nz,)),
            dma((nz,)),
            dma((2,)),
            dma((nz,)),
            dma((nz,)),
            dma((nz,)),
            dma((nz,)),
            dma((nz,)),
            dma((nz,)),
            dma((ntp,)),
            dma((ntp,)),
        ],
        compiler_params=pltpu.CompilerParams(
            collective_id=0, has_side_effects=True, vmem_limit_bytes=56 * 1024 * 1024
        ),
    )(normed, gx, gy, wx, wy, fx, fy, mx, my, sx, sy)

    n = min(8, R // 16)
    big, small = depth // n, R // n

    def block(rows, cols):
        return pl.BlockSpec((rows, cols), lambda k: (k, 0))

    def whole(rows, cols):
        return pl.BlockSpec((rows, cols), lambda k: (0, 0))

    return pl.pallas_call(
        functools.partial(output_kernel, 0.25 * math.sqrt(2.0 * depth * w * ntp)),
        grid=(n,),
        out_shape=[sds((R, w), F32)] * 4 + [sds((r, w), F32)] * 4 + [sds((depth, w), BF16)] * 2,
        in_specs=[
            pl.BlockSpec((2, big, rank), lambda k: (0, k, 0)),
            block(big, 2 * w),
            whole(rank, 2 * w),
            whole(r, 2 * w),
            whole(8, 128),
        ]
        + [block(small, w)] * 2
        + [block(small, rank)] * 2
        + [whole(r, w)] * 4,
        out_specs=[block(small, w)] * 4 + [whole(r, w)] * 4 + [block(big, w)] * 2,
        compiler_params=pltpu.CompilerParams(vmem_limit_bytes=40 * 1024 * 1024),
    )(f_full, w_full, d, low, tot, wx, wy, fx, fy, mx, my, sx, sy)


def solution(mesh):
    row, cut, rep = P("fs", None), P("fs", "tp"), P(None, "tp")
    return jax.shard_map(
        functools.partial(on_device, mesh.shape["fs"], mesh.shape["tp"]),
        mesh=mesh,
        in_specs=(row, cut, cut, cut, cut, row, row, cut, cut, cut, cut),
        out_specs=(cut,) * 8 + (rep, rep),
        check_vma=False,
    )
```

time: 261 us -> 105 us (0.40)
  waiting for transfers between devices: 167 us -> 0 us
  Pallas kernels: 0 us -> 96.9 us
  blocking collectives: 40.2 us -> 0 us
  matrix products: 17.5 us -> 0 us
  between operations: 15.9 us -> 0.79 us
  local copies, waits for them, and re-layouts: 15.1 us -> 7.25 us
  other arithmetic: 4.31 us -> 0 us
    pallas_call x0 -> x2, Pallas kernels: none -> 96.9 us  [the longest x1 89.4 us: on_device(): pl.pallas_call(functools.partial(exchange_kernel, nfs, ntp), out_shape=(s...]
    reduce_scatter x2 -> x0, waiting for transfers between devices: 87.4 us -> none  [the longest x1 52.8 us: on_device(): lax.psum_scatter(lax.dot_general(normed_in, cotangent, contract, preferre...]
    all_gather x3 -> x0, waiting for transfers between devices: 79.6 us -> none  [the longest x1 27.8 us: on_device(): lax.all_gather(new_x.astype(jnp.bfloat16), 'fs', axis=0, tiled=True)]
    psum x1 -> x0, blocking collectives: 40.2 us -> none  [on_device(): lax.psum(jnp.sum(update_x * update_x) + jnp.sum(update_y * update_y), ('f...]
    dot_general x5 -> x0, matrix products: 17.5 us -> none  [the longest x1 9.38 us: on_device(): lax.dot_general(normed_in, cotangent, contract, preferred_element_type=jn...]
    unnamed x23 -> x26, local copies, waits for them, and re-layouts: 15.1 us -> 7.25 us
  transfers between devices with their start and end apart: 5 -> 0, of which waited for: 5 -> 0; matrix products, arithmetic and copies ran while one was open for 4% -> 0% of each run, Pallas kernels for 0% -> 0%
where the time goes in v1:
time: 105 us
  Pallas kernels  96.9 us (92%)
  local copies, waits for them, and re-layouts  7.25 us (7%)
    pallas_call x1, Pallas kernels, on_device(): pl.pallas_call(functools.partial(exchange_kernel, nfs, ntp), out_shape=(s...  89.4 us
    pallas_call x1, Pallas kernels, on_device(): pl.pallas_call(functools.partial(output_kernel, 0.25 * math.sqrt(2.0 * de...  7.5 us
    unnamed x26, local copies, waits for them, and re-layouts  7.25 us

profile of v1, /device:TPU:0, one launch (start us, length us, event | category | flops | bytes accessed | tf_op | source)
XLA Modules:
  0.0 105.0 jit_solution(11598112548861053861)
XLA Ops:
  0.6 0.0 copy-start.10
  0.7 0.0 copy-start.9
  0.7 0.0 copy-start.8
  0.7 0.0 copy-start.7
  0.7 0.0 copy-start.5
  0.7 0.0 copy-start.4
  0.7 0.0 copy-start.3
  0.7 0.0 copy-start.2
  0.7 89.4 %shard_map.186 = (bf16[2,2048,512]{2,1,0:T(8,128)(2,1)}, bf16[2048,1024]{1,0:T(8,128)(2,1)}, bf16[512,1024]{1,0:T(8,128)(2,1)}, f32[64,1024]{1,0:T(8,128)}, f32[8,128]{1,0:T(8,128)}) custom-call(bf16[1024,2048]{1,0:T(8,128)(2,1)} %normed.1, bf16[1024,512]{1,0:T(8,128)(2,1)} %grad_x.1, bf16[1024,512]{1,0:T(8,128)(2,1)} %grad_y.1, f32[256,512]{1,0:T(8,128)} %weight_x.3, ...), custom_call_target="tpu_custom_call" | custom-call | tf_op jit(solution)/shard_map/pallas_call | solution.py:368
  90.2 0.0 copy-done.10
  90.2 0.0 copy-done.9
  90.2 0.0 copy-done.8
  90.2 0.0 copy-done.7
  90.2 0.0 copy-done.5
  90.2 0.0 copy-done.4
  90.2 0.0 copy-done.3
  90.2 0.0 copy-done.2
  90.2 0.0 copy-start
  90.3 2.2 %copy-done = bf16[2,2048,512]{2,1,0:T(8,128)(2,1)S(1)} copy-done((bf16[2,2048,512]{2,1,0:T(8,128)(2,1)S(1)}, bf16[2,2048,512]{2,1,0:T(8,128)(2,1)}, u32[]{:S(2)}) %copy-start) | copy-done | bytes 4194328
  92.4 2.2 %copy-done.1 = bf16[2048,1024]{1,0:T(8,128)(2,1)S(1)} copy-done((bf16[2048,1024]{1,0:T(8,128)(2,1)S(1)}, bf16[2048,1024]{1,0:T(8,128)(2,1)}, u32[]{:S(2)}) %copy-start.1) | copy-done | bytes 4194328
  94.6 1.2 %copy-done.6 = bf16[512,1024]{1,0:T(8,128)(2,1)S(1)} copy-done((bf16[512,1024]{1,0:T(8,128)(2,1)S(1)}, bf16[512,1024]{1,0:T(8,128)(2,1)}, u32[]{:S(2)}) %copy-start.6) | copy-done | bytes 1048600
  95.8 0.9 copy-done.11
  96.8 0.7 copy-done.12
  97.5 7.5 %shard_map.187 = (f32[256,512]{1,0:T(8,128)}, f32[256,512]{1,0:T(8,128)}, f32[256,512]{1,0:T(8,128)}, f32[256,512]{1,0:T(8,128)}, f32[64,512]{1,0:T(8,128)}, /*i...) custom-call(bf16[2,2048,512]{2,1,0:T(8,128)(2,1)S(1)} %copy-done, ...), custom_call_target="tpu_custom_call" | custom-call | tf_op jit(solution)/shard_map/pallas_call | solution.py:434
  (4 shorter events, 0.0 us)
Async XLA Ops:
  0.6 89.5 %copy-start.10 = (f32[64,512]{1,0:T(8,128)S(1)}, f32[64,512]{1,0:T(8,128)}, u32[]{:S(2)}) copy-start(f32[64,512]{1,0:T(8,128)} %second_y.3) | copy-start | bytes 393220
  0.7 89.5 %copy-start.9 = (f32[64,512]{1,0:T(8,128)S(1)}, f32[64,512]{1,0:T(8,128)}, u32[]{:S(2)}) copy-start(f32[64,512]{1,0:T(8,128)} %second_x.3) | copy-start | bytes 393220
  0.7 89.5 %copy-start.8 = (f32[64,512]{1,0:T(8,128)S(1)}, f32[64,512]{1,0:T(8,128)}, u32[]{:S(2)}) copy-start(f32[64,512]{1,0:T(8,128)} %first_y.3) | copy-start | bytes 393220
  0.7 89.5 %copy-start.7 = (f32[64,512]{1,0:T(8,128)S(1)}, f32[64,512]{1,0:T(8,128)}, u32[]{:S(2)}) copy-start(f32[64,512]{1,0:T(8,128)} %first_x.3) | copy-start | bytes 393220
  0.7 89.5 %copy-start.5 = (bf16[256,512]{1,0:T(8,128)(2,1)S(1)}, bf16[256,512]{1,0:T(8,128)(2,1)}, u32[]{:S(2)}) copy-start(bf16[256,512]{1,0:T(8,128)(2,1)} %factor_y.3) | copy-start | bytes 786436
  0.7 89.5 %copy-start.4 = (bf16[256,512]{1,0:T(8,128)(2,1)S(1)}, bf16[256,512]{1,0:T(8,128)(2,1)}, u32[]{:S(2)}) copy-start(bf16[256,512]{1,0:T(8,128)(2,1)} %factor_x.3) | copy-start | bytes 786436
  0.7 89.5 %copy-start.3 = (f32[256,512]{1,0:T(8,128)S(1)}, f32[256,512]{1,0:T(8,128)}, u32[]{:S(2)}) copy-start(f32[256,512]{1,0:T(8,128)} %weight_y.3) | copy-start | bytes 1572868
  0.7 89.5 %copy-start.2 = (f32[256,512]{1,0:T(8,128)S(1)}, f32[256,512]{1,0:T(8,128)}, u32[]{:S(2)}) copy-start(f32[256,512]{1,0:T(8,128)} %weight_x.3) | copy-start | bytes 1572868
  90.2 2.2 %copy-start = (bf16[2,2048,512]{2,1,0:T(8,128)(2,1)S(1)}, bf16[2,2048,512]{2,1,0:T(8,128)(2,1)}, u32[]{:S(2)}) copy-start(bf16[2,2048,512]{2,1,0:T(8,128)(2,1)} %get-tuple-element.15.f_full) | copy-start | bytes 12582916
  92.4 2.2 %copy-start.1 = (bf16[2048,1024]{1,0:T(8,128)(2,1)S(1)}, bf16[2048,1024]{1,0:T(8,128)(2,1)}, u32[]{:S(2)}) copy-start(bf16[2048,1024]{1,0:T(8,128)(2,1)} %get-tuple-element.16.w_full) | copy-start | bytes 12582916
  94.6 1.2 %copy-start.6 = (bf16[512,1024]{1,0:T(8,128)(2,1)S(1)}, bf16[512,1024]{1,0:T(8,128)(2,1)}, u32[]{:S(2)}) copy-start(bf16[512,1024]{1,0:T(8,128)(2,1)} %get-tuple-element.17.d) | copy-start | bytes 3145732
  95.8 0.9 copy-start.11
  96.8 0.7 copy-start.12

commit v2 on v1

--- a/solution.py
+++ b/solution.py
@@ -10,6 +10,7 @@
 
 MESH = pl.DeviceIdType.MESH
 F32, BF16 = jnp.float32, jnp.bfloat16
+PLACE = {"h": ((1, 0),), "scatter": ((1, 1), (2, 0)), "dir": ((2, 1),), "end": (("rest", 3),)}
 ROWS = (((0,), (0,)), ((), ()))
 
 
@@ -27,21 +28,19 @@
     first_y,
     second_x,
     second_y,
-    f_out,
+    f_buf,
     w_out,
-    d_out,
+    d_buf,
     low_out,
     tot_out,
     n_buf,
     gx_buf,
     gy_buf,
-    f_buf,
     h_buf,
     low,
     sib,
     rs_send,
     rs_recv,
-    d_buf,
     w_buf,
     w16,
     fm,
@@ -50,7 +49,6 @@
     g_lo,
     tot_recv,
     lsem,
-    bar_sem,
     f_line_s,
     f_line_r,
     f_tp_s,
@@ -143,29 +141,50 @@
     w16[...] = w_buf[...].astype(BF16)
     put = local(w16, w_out.at[rows(i, R)], 2)
 
-    def w_hop(step):
+    half = R // 2
+
+    def w_hop(step, part):
         for side, sign in ((0, 1), (1, -1)):
             src = z - sign * step
             nxt = z + sign
             has = (src >= 0) & (src < nz)
             to = has & (nxt >= 0) & (nxt < nz)
-            slot = w_out.at[rows(src * 2 + c, R)]
+            slot = w_out.at[rows((src * 2 + c) * 2 + part, half)]
 
             if step:
 
                 @pl.when(has)
                 def _():
-                    send(slot, slot, w_s.at[0, side], w_r.at[src], {"fs": o}).wait_recv()
-                    send(slot, slot, w_sib_s.at[src], w_sib_r.at[src], {"fs": o}).start()
+                    arrived = w_r.at[src, part]
+                    send(slot, slot, w_s.at[0, side, part], arrived, {"fs": o}).wait_recv()
 
             @pl.when(to)
             def _():
-                a = slot if step else w16
-                send(a, slot, w_s.at[step, side], w_r.at[src], {"fs": nxt * 2 + c}).start()
-
-    w_hop(0)
-    w_own = w_out.at[rows(i, R)]
-    go(send(w16, w_own, w_sib_s.at[z], w_sib_r.at[z], {"fs": o}))
+                a = slot if step else w16.at[pl.ds(part * half, half)]
+                there = {"fs": nxt * 2 + c}
+                send(a, slot, w_s.at[step, side, part], w_r.at[src, part], there).start()
+
+            if step:
+
+                @pl.when(has)
+                def _():
+                    sib_sems = w_sib_s.at[src, part], w_sib_r.at[src, part]
+                    send(slot, slot, *sib_sems, {"fs": o}).start()
+
+    def w_at(point):
+        for step, part in PLACE.get(point, ()):
+            if step == "rest":
+                for k in range(part, nz):
+                    w_hop(k, 0)
+                    w_hop(k, 1)
+            elif step < nz:
+                w_hop(step, part)
+
+    w_hop(0, 0)
+    w_hop(0, 1)
+    for part in range(2):
+        a, b = w16.at[pl.ds(part * half, half)], w_out.at[rows(i * 2 + part, half)]
+        go(send(a, b, w_sib_s.at[z, part], w_sib_r.at[z, part], {"fs": o}))
 
     for k in range(1, nz):
         zs = lax.rem(z + nz - k, nz)
@@ -188,8 +207,8 @@
         for v in range(q):
             p = piece(zs * 2 + 1 - c, v)
             send(p, p, f_sib_s.at[zs, v], f_sib_r.at[zs, v], {"fs": o}).wait_recv()
-    keep_f = local(f_buf, f_out, 0)
-
+
+    w_at("factors")
     for cp in cps_n:
         cp.wait()
     tile = min(256, tokens)
@@ -201,6 +220,7 @@
             h = jnp.dot(a, f_buf[b], preferred_element_type=F32)
             h_buf[rows(k, tile), pl.ds(b * rank, rank)] = h.astype(BF16)
 
+    w_at("h")
     lanes = 128
     m = lanes // (2 * r)
 
@@ -211,6 +231,7 @@
             part = lax.dot_general(h, g[...], ROWS, preferred_element_type=F32)
             low[pl.ds(k * m, m), :, :, pl.ds(b * w, w)] = part.reshape(m, 2, r, w)
 
+    w_at("low")
     go(send(low.at[:, 1 - c], sib, sib_s.at[0], sib_s.at[1], {"fs": o}))
     sent[-1].wait_recv()
     for k in range(1, nz):
@@ -218,8 +239,7 @@
         rs_send[zd] = (low[zd, c] + sib[zd]).astype(BF16)
         go(send(rs_send.at[zd], rs_recv.at[z], rs_s.at[k], rs_r.at[z], {"fs": zd * 2 + c}))
 
-    for step in range(1, nz - 1):
-        w_hop(step)
+    w_at("scatter")
 
     @pl.loop(0, rank // lanes)
     def _(k):
@@ -230,6 +250,7 @@
             g_hi[b, rows(k, lanes), :] = hi
             g_lo[b, rows(k, lanes), :] = (gram - hi.astype(F32)).astype(BF16)
 
+    w_at("gram")
     for cp in cps_m:
         cp.wait()
     total = low[z, c] + sib[z]
@@ -242,11 +263,13 @@
     ns = 0.9 * sm[...] + 0.1 * total * total
     d_buf[rows(i, r), :] = (nf / jnp.sqrt(ns)).astype(BF16)
 
+    w_at("predir")
     d_own = d_buf.at[rows(i, r)]
     for k in range(1, nz):
         zd = lax.rem(z + k, nz)
         go(send(d_own, d_own, d_line_s.at[k], d_line_r.at[z], {"fs": zd * 2 + c}))
     go(send(d_own, d_own, d_sib_s.at[z], d_sib_r.at[z], {"fs": o}))
+    w_at("dir")
     for k in range(1, nz):
         zs = lax.rem(z + k, nz)
         p = d_buf.at[rows(zs * 2 + c, r)]
@@ -256,8 +279,8 @@
         zs = lax.rem(z + k, nz)
         p = d_buf.at[rows(zs * 2 + 1 - c, r)]
         send(p, p, d_sib_s.at[zs], d_sib_r.at[zs], {"fs": o}).wait_recv()
-    keep_d = local(d_buf, d_out, 1)
-
+
+    w_at("gathered")
     part = 0.0
     for b in range(2):
         d = d_buf[:, pl.ds(b * w, w)]
@@ -269,8 +292,7 @@
         slot = tot_recv.at[t]
         go(send(slot, slot, t_s.at[k], t_r.at[t], {"tp": lax.rem(t + k, ntp)}))
 
-    if nz > 1:
-        w_hop(nz - 1)
+    w_at("end")
 
     acc = tot_recv[t]
     for k in range(1, ntp):
@@ -280,29 +302,29 @@
         acc = acc + tot_recv[ts]
     tot_out[...] = acc
 
-    for zs in range(nz):
-        slot = w_out.at[pl.ds((zs * 2) * R, R)]
-        send(slot, slot, w_sib_s.at[zs], w_sib_r.at[zs], {"fs": o}).wait_recv()
-
-        @pl.when(zs != z)
-        def _():
-            send(slot, slot, w_sib_s.at[zs], w_sib_r.at[zs], {"fs": o}).wait_send()
-
-    for step in range(nz - 1):
-        for side, sign in ((0, 1), (1, -1)):
-            src = z - sign * step
-            nxt = z + sign
-
-            @pl.when((src >= 0) & (src < nz) & (nxt >= 0) & (nxt < nz))
+    for part in range(2):
+        for zs in range(nz):
+            slot = w_out.at[pl.ds(zs * 2 * R, half)]
+            done = send(slot, slot, w_sib_s.at[zs, part], w_sib_r.at[zs, part], {"fs": o})
+            done.wait_recv()
+
+            @pl.when(zs != z)
             def _():
-                a = w_out.at[rows(src * 2 + c, R)] if step else w16
-                send(a, a, w_s.at[step, side], w_r.at[0], {"fs": o}).wait_send()
+                done.wait_send()
+
+        for step in range(nz - 1):
+            for side, sign in ((0, 1), (1, -1)):
+                src = z - sign * step
+                nxt = z + sign
+
+                @pl.when((src >= 0) & (src < nz) & (nxt >= 0) & (nxt < nz))
+                def _():
+                    a = w16.at[pl.ds(0, half)]
+                    send(a, a, w_s.at[step, side, part], w_r.at[0, part], {"fs": o}).wait_send()
 
     for cp in sent:
         cp.wait_send()
     put.wait()
-    keep_f.wait()
-    keep_d.wait()
 
 
 def output_kernel(
@@ -368,25 +390,23 @@
     f_full, w_full, d, low, tot = pl.pallas_call(
         functools.partial(exchange_kernel, nfs, ntp),
         out_shape=(
-            sds((2, depth, rank), BF16),
-            sds((depth, 2 * w), BF16),
-            sds((rank, 2 * w), BF16),
-            sds((r, 2 * w), F32),
-            sds((8, 128), F32),
+            V((2, depth, rank), BF16),
+            V((depth, 2 * w), BF16),
+            V((rank, 2 * w), BF16),
+            V((r, 2 * w), F32),
+            V((8, 128), F32),
         ),
         in_specs=[anyspec] * 11,
-        out_specs=(anyspec, anyspec, anyspec, vmem, vmem),
+        out_specs=(vmem,) * 5,
         scratch_shapes=[
             V((tokens, depth), BF16),
             V((tokens, w), BF16),
             V((tokens, w), BF16),
-            V((2, depth, rank), BF16),
             V((tokens, 2 * rank), BF16),
             V((nz, 2, r, 2 * w), F32),
             V((nz, r, 2 * w), F32),
             V((nz, r, 2 * w), BF16),
             V((nz, r, 2 * w), BF16),
-            V((rank, 2 * w), BF16),
             V((R, 2 * w), F32),
             V((R, 2 * w), BF16),
             V((r, 2 * w), F32),
@@ -395,7 +415,6 @@
             V((2, rank, rank), BF16),
             V((ntp, 8, 128), F32),
             dma((11,)),
-            pltpu.SemaphoreType.REGULAR,
             dma((nz,)),
             dma((nz,)),
             dma((nz, q)),
@@ -403,10 +422,10 @@
             dma((nz, q)),
             dma((nz, q)),
             dma((1,)),
+            dma((nz, 2, 2)),
             dma((nz, 2)),
-            dma((nz,)),
-            dma((nz,)),
-            dma((nz,)),
+            dma((nz, 2)),
+            dma((nz, 2)),
             dma((2,)),
             dma((nz,)),
             dma((nz,)),
@@ -418,7 +437,7 @@
             dma((ntp,)),
         ],
         compiler_params=pltpu.CompilerParams(
-            collective_id=0, has_side_effects=True, vmem_limit_bytes=56 * 1024 * 1024
+            collective_id=0, has_side_effects=True, vmem_limit_bytes=48 * 1024 * 1024
         ),
     )(normed, gx, gy, wx, wy, fx, fy, mx, my, sx, sy)
 

time: 105 us -> 85.9 us (0.82)
  Pallas kernels: 96.9 us -> 85 us
  local copies, waits for them, and re-layouts: 7.25 us -> 0.03 us
    pallas_call x1, Pallas kernels: 89.4 us -> 77.4 us  [on_device(): pl.pallas_call(functools.partial(exchange_kernel, nfs, ntp), out_shape=(V...]
    unnamed x26 -> x16, local copies, waits for them, and re-layouts: 7.25 us -> 0.03 us
where the time goes in v2:
time: 85.9 us; the launch traced here: 85.8 us
  Pallas kernels  85 us (99%)
    pallas_call x1, Pallas kernels, on_device(): pl.pallas_call(functools.partial(exchange_kernel, nfs, ntp), out_shape=(V...  77.4 us
    pallas_call x1, Pallas kernels, on_device(): pl.pallas_call(functools.partial(output_kernel, 0.25 * math.sqrt(2.0 * de...  7.53 us

profile of v2, /device:TPU:0, one launch (start us, length us, event | category | flops | bytes accessed | tf_op | source)
XLA Modules:
  0.0 85.8 jit_solution(15149944230119166016)
XLA Ops:
  0.6 0.0 copy-start.7
  0.7 0.0 copy-start.6
  0.7 0.0 copy-start.5
  0.7 0.0 copy-start.4
  0.7 0.0 copy-start.3
  0.7 0.0 copy-start.2
  0.7 0.0 copy-start.1
  0.7 0.0 copy-start
  0.7 77.4 %shard_map.186 = (bf16[2,2048,512]{2,1,0:T(8,128)(2,1)S(1)}, bf16[2048,1024]{1,0:T(8,128)(2,1)S(1)}, bf16[512,1024]{1,0:T(8,128)(2,1)S(1)}, f32[64,1024]{1,0:T(8,128)S(1)}, f32[8,128]{1,0:T(8,128)S(1)}) custom-call(bf16[1024,2048]{1,0:T(8,128)(2,1)} %normed.1, bf16[1024,512]{1,0:T(8,128)(2,1)} %grad_x.1, bf16[1024,512]{1,0:T(8,128)(2,1)} %grad_y.1, ...), custom_call_target="tpu_custom_call" | custom-call | tf_op jit(solution)/shard_map/pallas_call | solution.py:390
  78.2 0.0 copy-done.7
  78.2 0.0 copy-done.6
  78.2 0.0 copy-done.5
  78.2 0.0 copy-done.4
  78.2 0.0 copy-done.3
  78.2 0.0 copy-done.2
  78.2 0.0 copy-done.1
  78.2 0.0 copy-done
  78.2 7.5 %shard_map.187 = (f32[256,512]{1,0:T(8,128)}, f32[256,512]{1,0:T(8,128)}, f32[256,512]{1,0:T(8,128)}, f32[256,512]{1,0:T(8,128)}, f32[64,512]{1,0:T(8,128)}, /*i...) custom-call(bf16[2,2048,512]{2,1,0:T(8,128)(2,1)S(1)} %get-tuple-ele, ...), custom_call_target="tpu_custom_call" | custom-call | tf_op jit(solution)/shard_map/pallas_call | solution.py:453
Async XLA Ops:
  0.6 77.5 %copy-start.7 = (f32[64,512]{1,0:T(8,128)S(1)}, f32[64,512]{1,0:T(8,128)}, u32[]{:S(2)}) copy-start(f32[64,512]{1,0:T(8,128)} %second_y.3) | copy-start | bytes 393220
  0.7 77.5 %copy-start.6 = (f32[64,512]{1,0:T(8,128)S(1)}, f32[64,512]{1,0:T(8,128)}, u32[]{:S(2)}) copy-start(f32[64,512]{1,0:T(8,128)} %second_x.3) | copy-start | bytes 393220
  0.7 77.5 %copy-start.5 = (f32[64,512]{1,0:T(8,128)S(1)}, f32[64,512]{1,0:T(8,128)}, u32[]{:S(2)}) copy-start(f32[64,512]{1,0:T(8,128)} %first_y.3) | copy-start | bytes 393220
  0.7 77.5 %copy-start.4 = (f32[64,512]{1,0:T(8,128)S(1)}, f32[64,512]{1,0:T(8,128)}, u32[]{:S(2)}) copy-start(f32[64,512]{1,0:T(8,128)} %first_x.3) | copy-start | bytes 393220
  0.7 77.5 %copy-start.3 = (bf16[256,512]{1,0:T(8,128)(2,1)S(1)}, bf16[256,512]{1,0:T(8,128)(2,1)}, u32[]{:S(2)}) copy-start(bf16[256,512]{1,0:T(8,128)(2,1)} %factor_y.3) | copy-start | bytes 786436
  0.7 77.5 %copy-start.2 = (bf16[256,512]{1,0:T(8,128)(2,1)S(1)}, bf16[256,512]{1,0:T(8,128)(2,1)}, u32[]{:S(2)}) copy-start(bf16[256,512]{1,0:T(8,128)(2,1)} %factor_x.3) | copy-start | bytes 786436
  0.7 77.5 %copy-start.1 = (f32[256,512]{1,0:T(8,128)S(1)}, f32[256,512]{1,0:T(8,128)}, u32[]{:S(2)}) copy-start(f32[256,512]{1,0:T(8,128)} %weight_y.3) | copy-start | bytes 1572868
  0.7 77.5 %copy-start = (f32[256,512]{1,0:T(8,128)S(1)}, f32[256,512]{1,0:T(8,128)}, u32[]{:S(2)}) copy-start(f32[256,512]{1,0:T(8,128)} %weight_x.3) | copy-start | bytes 1572868

commit v3 on v2

--- a/solution.py
+++ b/solution.py
@@ -10,7 +10,7 @@
 
 MESH = pl.DeviceIdType.MESH
 F32, BF16 = jnp.float32, jnp.bfloat16
-PLACE = {"h": ((1, 0),), "scatter": ((1, 1), (2, 0)), "dir": ((2, 1),), "end": (("rest", 3),)}
+PLACE = {"factors": ((1, 0),), "h": ((1, 1),), "scatter": ((2, 0),), "gram": ((2, 1),), "end": (("rest", 3),)}
 ROWS = (((0,), (0,)), ((), ()))
 
 
@@ -355,6 +355,8 @@
 ):
     scale = jnp.minimum(1.0, scale_top / jnp.sqrt(tot[0:1, 0:1]))
     w = weight_x.shape[1]
+    big = copy_x.shape[0]
+    now = pl.ds(pl.multiple_of(pl.program_id(0) * big, big), big)
     sides = (
         (factor_x, weight_x, first_x, second_x, new_x, step_x, nf_x, ns_x, copy_x),
         (factor_y, weight_y, first_y, second_y, new_y, step_y, nf_y, ns_y, copy_y),
@@ -362,8 +364,8 @@
     for b, (factor, weight, first, second, new, step, nf, ns, copy) in enumerate(sides):
         cols = pl.ds(b * w, w)
         db = d[:, cols]
-        up = jnp.dot(f_full[b], db, preferred_element_type=F32)
-        copy[...] = (w_full[:, cols].astype(F32) - 0.02 * (scale * up)).astype(BF16)
+        up = jnp.dot(f_full[b, now, :], db, preferred_element_type=F32)
+        copy[...] = (w_full[now, cols].astype(F32) - 0.02 * (scale * up)).astype(BF16)
         st = scale * jnp.dot(factor[...], db, preferred_element_type=F32)
         step[...] = st
         new[...] = weight[...] - 0.02 * st
@@ -441,7 +443,7 @@
         ),
     )(normed, gx, gy, wx, wy, fx, fy, mx, my, sx, sy)
 
-    n = min(8, R // 16)
+    n = min(4, R // 16)
     big, small = depth // n, R // n
 
     def block(rows, cols):
@@ -455,9 +457,9 @@
         grid=(n,),
         out_shape=[sds((R, w), F32)] * 4 + [sds((r, w), F32)] * 4 + [sds((depth, w), BF16)] * 2,
         in_specs=[
-            pl.BlockSpec((2, big, rank), lambda k: (0, k, 0)),
-            block(big, 2 * w),
-            whole(rank, 2 * w),
+            vmem,
+            vmem,
+            vmem,
             whole(r, 2 * w),
             whole(8, 128),
         ]

time: 85.9 us -> 83.7 us (0.974)
  Pallas kernels: 85 us -> 82.7 us
    pallas_call x1, Pallas kernels: 7.53 us -> 5.76 us  [on_device(): pl.pallas_call(functools.partial(output_kernel, 0.25 * math.sqrt(2.0 * de...]
where the time goes in v3:
time: 83.7 us; the launch traced here: 83.5 us
  Pallas kernels  82.7 us (99%)
    pallas_call x1, Pallas kernels, on_device(): pl.pallas_call(functools.partial(exchange_kernel, nfs, ntp), out_shape=(V...  77 us
    pallas_call x1, Pallas kernels, on_device(): pl.pallas_call(functools.partial(output_kernel, 0.25 * math.sqrt(2.0 * de...  5.76 us

profile of v3, /device:TPU:0, one launch (start us, length us, event | category | flops | bytes accessed | tf_op | source)
XLA Modules:
  0.0 83.5 jit_solution(17675789698653807610)
XLA Ops:
  0.6 0.0 copy-start.7
  0.7 0.0 copy-start.6
  0.7 0.0 copy-start.5
  0.7 0.0 copy-start.4
  0.7 0.0 copy-start.3
  0.7 0.0 copy-start.2
  0.7 0.0 copy-start.1
  0.7 0.0 copy-start
  0.7 77.0 %shard_map.186 = (bf16[2,2048,512]{2,1,0:T(8,128)(2,1)S(1)}, bf16[2048,1024]{1,0:T(8,128)(2,1)S(1)}, bf16[512,1024]{1,0:T(8,128)(2,1)S(1)}, f32[64,1024]{1,0:T(8,128)S(1)}, f32[8,128]{1,0:T(8,128)S(1)}) custom-call(bf16[1024,2048]{1,0:T(8,128)(2,1)} %normed.1, bf16[1024,512]{1,0:T(8,128)(2,1)} %grad_x.1, bf16[1024,512]{1,0:T(8,128)(2,1)} %grad_y.1, ...), custom_call_target="tpu_custom_call" | custom-call | tf_op jit(solution)/shard_map/pallas_call | solution.py:392
  77.7 0.0 copy-done.7
  77.7 0.0 copy-done.6
  77.7 0.0 copy-done.5
  77.7 0.0 copy-done.4
  77.7 0.0 copy-done.3
  77.7 0.0 copy-done.2
  77.7 0.0 copy-done.1
  77.8 0.0 copy-done
  77.8 5.8 %shard_map.187 = (f32[256,512]{1,0:T(8,128)}, f32[256,512]{1,0:T(8,128)}, f32[256,512]{1,0:T(8,128)}, f32[256,512]{1,0:T(8,128)}, f32[64,512]{1,0:T(8,128)}, /*i...) custom-call(bf16[2,2048,512]{2,1,0:T(8,128)(2,1)S(1)} %get-tuple-ele, ...), custom_call_target="tpu_custom_call" | custom-call | tf_op jit(solution)/shard_map/pallas_call | solution.py:455
Async XLA Ops:
  0.6 77.0 %copy-start.7 = (f32[64,512]{1,0:T(8,128)S(1)}, f32[64,512]{1,0:T(8,128)}, u32[]{:S(2)}) copy-start(f32[64,512]{1,0:T(8,128)} %second_y.3) | copy-start | bytes 393220
  0.7 77.0 %copy-start.6 = (f32[64,512]{1,0:T(8,128)S(1)}, f32[64,512]{1,0:T(8,128)}, u32[]{:S(2)}) copy-start(f32[64,512]{1,0:T(8,128)} %second_x.3) | copy-start | bytes 393220
  0.7 77.0 %copy-start.5 = (f32[64,512]{1,0:T(8,128)S(1)}, f32[64,512]{1,0:T(8,128)}, u32[]{:S(2)}) copy-start(f32[64,512]{1,0:T(8,128)} %first_y.3) | copy-start | bytes 393220
  0.7 77.0 %copy-start.4 = (f32[64,512]{1,0:T(8,128)S(1)}, f32[64,512]{1,0:T(8,128)}, u32[]{:S(2)}) copy-start(f32[64,512]{1,0:T(8,128)} %first_x.3) | copy-start | bytes 393220
  0.7 77.0 %copy-start.3 = (bf16[256,512]{1,0:T(8,128)(2,1)S(1)}, bf16[256,512]{1,0:T(8,128)(2,1)}, u32[]{:S(2)}) copy-start(bf16[256,512]{1,0:T(8,128)(2,1)} %factor_y.3) | copy-start | bytes 786436
  0.7 77.0 %copy-start.2 = (bf16[256,512]{1,0:T(8,128)(2,1)S(1)}, bf16[256,512]{1,0:T(8,128)(2,1)}, u32[]{:S(2)}) copy-start(bf16[256,512]{1,0:T(8,128)(2,1)} %factor_x.3) | copy-start | bytes 786436
  0.7 77.0 %copy-start.1 = (f32[256,512]{1,0:T(8,128)S(1)}, f32[256,512]{1,0:T(8,128)}, u32[]{:S(2)}) copy-start(f32[256,512]{1,0:T(8,128)} %weight_y.3) | copy-start | bytes 1572868
  0.7 77.0 %copy-start = (f32[256,512]{1,0:T(8,128)S(1)}, f32[256,512]{1,0:T(8,128)}, u32[]{:S(2)}) copy-start(f32[256,512]{1,0:T(8,128)} %weight_x.3) | copy-start | bytes 1572868
